TPU v7x, 256 devices: a whole 4x4x8 slice. The times are simulated.
256 devices in a mesh: ep: 64 (over z, y, core), tp: 4 (over x).
Axes of the slice: x: 4, y: 4, z: 8, core: 2. Of those that a mesh axis runs over, the one named last changes fastest.
Arguments:
- tokens: bfloat16 [49152, 2048], P('ep', 'tp')
- norm_gain: float32 [2048], P('tp'), may hold values from 0.1 to 1.9
- routing: int32 [49152, 2], P('ep'), may hold values from 0 to 63, as said below
- route_weight: float32 [49152, 2], P('ep'), may hold values from 0.2 to 1
- w_gate: bfloat16 [64, 2048, 512], P('ep', 'tp'), may hold values from -0.125 to 0.125
- w_up: bfloat16 [64, 2048, 512], P('ep', 'tp'), may hold values from -0.125 to 0.125
- w_down: bfloat16 [64, 512, 2048], P('ep', None, 'tp'), may hold values from -0.25 to 0.25
- w_branch_in: bfloat16 [2048, 1024], P('ep', 'tp'), may hold values from -0.125 to 0.125
- w_branch_out: bfloat16 [1024, 2048], P('tp', 'ep'), may hold values from -0.1875 to 0.1875
- branch_gate: float32 [2048], P('tp'), may hold values from -3 to 3
Outputs:
- mixed: bfloat16 [49152, 2048], P('ep', 'tp')
Inputs may be any that keep to these rules, and one draw needn't show every extreme that they name: `routing`: each row names two different experts of the same group; expert e belongs to group e // 16. Among the rows of one device (aligned blocks of 768 rows) no expert is named more than 48 times, and in every block all experts of one group are named exactly 48 times.
All inputs are finite; a program needn't handle non-finite values.
Results may differ from a plain program's by a relative error of at most 0.0069.
Values may be sent and summed in bfloat16 or wider, within the bound.
A program may use at most 128 MiB of HBM per device.

v0:
```python
import jax
import jax.numpy as jnp
from jax import lax
from jax.sharding import PartitionSpec as P

GROUPS = 4
epsilon = 1e-06


def sent_to_all(value, axis):
    size = lax.axis_size(axis)
    return lax.all_to_all(
        jnp.broadcast_to(value[None], (size, *value.shape)), axis, 0, 0, tiled=True
    )


def taken_together(value, axis):
    return sent_to_all(value, axis).sum(axis=0)


def gather_turned(arrays, axis, dims):
    turned = [jnp.moveaxis(a, dim, 0) for a, dim in zip(arrays, dims)]
    both = jnp.concatenate([t.reshape(len(t), -1) for t in turned], axis=1)
    filled, at, gathered = (lax.all_gather(both, axis, axis=0, tiled=True), 0, [])
    for t, dim in zip(turned, dims):
        share = filled[:, at : at + t[0].size].reshape(-1, *t.shape[1:])
        gathered.append(jnp.moveaxis(share, 0, dim))
        at += t[0].size
    return tuple(gathered)


def send_back(result):
    return lax.all_to_all(result, "ep", split_axis=0, concat_axis=0, tiled=True)


def body(
    tokens,
    norm_gain,
    routing,
    route_weight,
    w_gate,
    w_up,
    w_down,
    w_branch_in,
    w_branch_out,
    branch_gate,
):
    token_count, quarter = tokens.shape
    full_width = quarter * lax.axis_size("tp")
    floats = tokens.astype(jnp.float32)
    squares = taken_together(jnp.sum(floats * floats, axis=1), "tp")
    normed = (floats * lax.rsqrt(squares[:, None] / full_width + epsilon) * norm_gain).astype(
        jnp.bfloat16
    )
    expert_count = lax.axis_size("ep") * w_gate.shape[0]
    capacity = token_count // (expert_count // GROUPS)
    flat_ids = routing.reshape(-1)
    one_hot = (flat_ids[:, None] == jnp.arange(expert_count, dtype=jnp.int32)[None, :]).astype(
        jnp.int32
    )
    before = jnp.cumsum(one_hot, axis=0) - one_hot
    position = flat_ids * capacity + jnp.sum(before * one_hot, axis=1)
    copies = jnp.repeat(normed, 2, axis=0)
    buffer = jnp.zeros((expert_count * capacity, quarter), jnp.bfloat16).at[position].set(copies)
    buffer = buffer.reshape(expert_count, capacity, quarter)
    gate_whole, up_whole, down_whole = (
        lax.all_gather(w_gate[0], "tp", axis=0, tiled=True),
        lax.all_gather(w_up[0], "tp", axis=0, tiled=True),
        lax.all_gather(w_down[0], "tp", axis=1, tiled=True),
    )
    row_split = lax.all_to_all(
        lax.all_to_all(buffer, "ep", split_axis=0, concat_axis=0, tiled=True),
        "tp",
        split_axis=0,
        concat_axis=2,
        tiled=True,
    )
    slot_rows = row_split.reshape(-1, row_split.shape[2])
    gate_sum = jnp.dot(slot_rows, gate_whole, preferred_element_type=jnp.float32)
    up_sum = jnp.dot(slot_rows, up_whole, preferred_element_type=jnp.float32)
    hidden = (jax.nn.silu(gate_sum) * up_sum).astype(jnp.bfloat16)
    result = jnp.dot(hidden, down_whole, preferred_element_type=jnp.float32).astype(jnp.bfloat16)
    feature_split = lax.all_to_all(
        result.reshape(row_split.shape), "tp", split_axis=2, concat_axis=0, tiled=True
    )
    returned = send_back(feature_split)
    picked = returned.reshape(expert_count * capacity, quarter)[position].reshape(
        token_count, 2, quarter
    )
    routed = jnp.sum(picked.astype(jnp.float32) * route_weight[:, :, None], axis=1)
    branch_tokens = lax.all_to_all(normed, "tp", split_axis=0, concat_axis=1, tiled=True)
    in_cols, out_rows = gather_turned((w_branch_in, w_branch_out), "tp", (1, 0))
    in_whole, out_whole = gather_turned((in_cols, out_rows), "ep", (0, 1))
    branch_hidden = jax.nn.silu(
        jnp.dot(branch_tokens, in_whole, preferred_element_type=jnp.float32)
    ).astype(jnp.bfloat16)
    branch_local = jnp.dot(branch_hidden, out_whole, preferred_element_type=jnp.float32).astype(
        jnp.bfloat16
    )
    branch = lax.all_to_all(branch_local, "tp", split_axis=1, concat_axis=0, tiled=True)
    return (routed + jax.nn.sigmoid(branch_gate) * branch.astype(jnp.float32)).astype(jnp.bfloat16)


def solution(mesh):
    return jax.shard_map(
        body,
        mesh=mesh,
        in_specs=(
            P("ep", "tp"),
            P("tp"),
            P("ep", None),
            P("ep", None),
            P("ep", "tp", None),
            P("ep", "tp", None),
            P("ep", None, "tp"),
            P("ep", "tp"),
            P("tp", "ep"),
            P("tp"),
        ),
        out_specs=P("ep", "tp"),
        check_vma=False,
    )
```

profile of v0, /device:TPU:2, one launch (start us, length us, event | category | flops | bytes accessed | tf_op | source)
XLA Modules:
  0.0 391.7 jit_solution(14819414351238019944)
XLA Ops:
  6.5 0.7 all-gather.10.cloned.1.call-update
  8.0 1.4 fusion.12
  10.0 5.5 %all-to-all-start = ((f32[4,1,768]{2,1,0:T(1,128)}), f32[4,1,768]{2,1,0:T(1,128)S(1)}, u32[]{:S(2)}, u32[]{:S(2)}) async-start(f32[4,1,768]{2,1,0:T(1,128)} %broadcast_in_dim.7), calls=%async_computation | async-start | bytes 24576 | tf_op jit(solution)/shard_map/all_to_all | solution.py:12
  15.4 0.7 all-gather.14.cloned.1.call-update
  16.9 18.1 %reduce-window.6 = s32[64,12,128]{2,1,0:T(8,128)S(1)} reduce-window(s32[64,12,128]{2,1,0:T(8,128)S(1)} %fusion.27, s32[]{:T(128)} %constant.6.clone.1), window={size=1x1x128 pad=0_0x0_0x127_0}, to_apply=%region_0.0 | reduce-window | flops 12484608 | bytes 786436 | tf_op jit(solution)/shard_map/reduce-window
  36.8 0.9 copy-done
  37.7 0.8 broadcast_in_dim.8
  39.2 9.5 %scatter_custom_fusion = bf16[3072,512]{1,0:T(8,128)(2,1)} fusion(s32[1536]{0:T(1024)S(1)} %fusion.32, bf16[1536,512]{1,0:T(8,128)(2,1)S(1)} %reshape.110, bf16[]{:T(256)} %constant.8.clone.1), kind=kCustom, calls=%fused_computation.23 | custom fusion | bytes 3145730 | tf_op jit(solution)/shard_map/scatter | solution.py:64
  48.7 11.6 %all-to-all-start.1 = ((bf16[64,48,512]{2,1,0:T(8,128)(2,1)}), bf16[64,48,512]{2,1,0:T(8,128)(2,1)S(1)}, u32[]{:S(2)}, u32[]{:S(2)}) async-start(bf16[64,48,512]{2,1,0:T(8,128)(2,1)} %bitcast.74), calls=%async_computation.1 | async-start | bytes 6291456 | tf_op jit(solution)/shard_map/all_to_all | solution.py:72
  60.4 12.7 %all_gather.18 = bf16[1024,64]{0,1:T(8,128)(2,1)S(1)} all-gather(bf16[256,64]{0,1:T(8,128)(2,1)S(1)} %pad_maximum_fusion.1), channel_id=1, replica_groups=mesh['ep'=64,'tp'=4] {'tp'}, dimensions={0}, use_global_device_ids=true | all-gather | bytes 163840 | tf_op jit(solution)/shard_map/all_gather | solution.py:24
  73.7 60.4 %all-to-all-done.1 = bf16[64,48,512]{2,1,0:T(8,128)(2,1)S(1)} async-done(((bf16[64,48,512]{2,1,0:T(8,128)(2,1)}), bf16[64,48,512]{2,1,0:T(8,128)(2,1)S(1)}, u32[]{:S(2)}, u32[]{:S(2)}) %all-to-all-start.1) | async-done | bytes 3145760 | tf_op jit(solution)/shard_map/all_to_all | solution.py:72
  134.2 39.5 %all_to_all.81 = bf16[64,48,512]{2,1,0:T(8,128)(2,1)S(1)} all-to-all(bf16[64,48,512]{2,1,0:T(8,128)(2,1)S(1)} %all-to-all-done.1), channel_id=1, replica_groups=mesh['ep'=64,'tp'=4] {'tp'}, dimensions={0} | all-to-all | bytes 6291456 | tf_op jit(solution)/shard_map/all_to_all | solution.py:71
  173.6 2.6 copy.61
  176.3 1.0 copy.71
  177.3 4.6 %fusion.10 = f32[768,512]{1,0:T(8,128)} fusion(bf16[768,2048]{1,0:T(8,128)(2,1)S(1)} %bitcast.79, bf16[1,2048,512]{2,1,0:T(8,128)(2,1)} %all-gather.10.cloned.1.call-done), kind=kOutput, calls=%fused_computation.12 | convolution fusion | flops 1610612736 | bytes 6815744 | tf_op jit(solution)/shard_map/dot_general | solution.py:79
  182.0 7.9 %convolution_convert_fusion = bf16[768,2048]{1,0:T(8,128)(2,1)} fusion(bf16[1,512,2048]{2,1,0:T(8,128)(2,1)} %all-gather.14.cloned.1.call-done, f32[768,512]{1,0:T(8,128)} %fusion.10, bf16[768,2048]{1,0:T(8,128)(2,1)S(1)} %bitcast.80, bf16[1,2048,512]{2,1,0:T(8,128)(2,1)} %all-gather.12.cloned.1.call-done), kind=kOutput, calls=%fused_computation.6 | convolution fusion | flops 3225157632 | bytes 12058624 | tf_op jit(solution)/shard_map/dot_general | solution.py:82
  189.9 10.5 %copy.62 = bf16[16,48,2048]{1,0,2:T(8,128)(2,1)} copy(bf16[16,48,2048]{2,1,0:T(8,128)(2,1)} %bitcast.82) | data formatting | bytes 6291456 | tf_op jit(solution)/shard_map/reshape | solution.py:84
  200.4 14.8 %reshape.120 = bf16[4,2,196608]{2,1,0:T(2,128)(2,1)} reshape(bf16[2048,16,48]{2,1,0:T(8,128)(2,1)} %bitcast.72) | data formatting | bytes 6291456
  215.2 38.8 %all_to_all.82 = bf16[4,2,196608]{2,1,0:T(2,128)(2,1)S(1)} all-to-all(bf16[4,2,196608]{2,1,0:T(2,128)(2,1)} %reshape.120), channel_id=1, replica_groups=mesh['ep'=64,'tp'=4] {'tp'}, dimensions={0} | all-to-all | bytes 6291456 | tf_op jit(solution)/shard_map/all_to_all | solution.py:83
  254.0 5.6 %all-to-all-start.5 = ((bf16[4,192,512]{2,1,0:T(8,128)(2,1)}), bf16[4,192,512]{2,1,0:T(8,128)(2,1)}, u32[]{:S(2)}, u32[]{:S(2)}) async-start(bf16[4,192,512]{2,1,0:T(8,128)(2,1)} %bitcast.78), calls=%async_computation.5 | async-start | bytes 1572864 | tf_op jit(solution)/shard_map/all_to_all | solution.py:91
  259.6 9.9 %reshape.121 = bf16[2048,16,48]{2,1,0:T(8,128)(2,1)} reshape(bf16[4,2,196608]{2,1,0:T(2,128)(2,1)S(1)} %all_to_all.82) | data formatting | bytes 6291456
  269.5 9.5 %copy.63 = bf16[4,16,48,512]{3,2,1,0:T(8,128)(2,1)} copy(bf16[4,16,48,512]{2,1,3,0:T(8,128)(2,1)} %bitcast.73) | data formatting | bytes 6291456 | tf_op jit(solution)/shard_map/all_to_all | solution.py:83
  279.1 9.2 %all-to-all-start.4 = ((bf16[64,48,512]{2,1,0:T(8,128)(2,1)}), bf16[64,48,512]{2,1,0:T(8,128)(2,1)S(1)}, u32[]{:S(2)}, u32[]{:S(2)}) async-start(bf16[64,48,512]{2,1,0:T(8,128)(2,1)} %bitcast.77), calls=%async_computation.4 | async-start | bytes 6291456 | tf_op jit(solution)/shard_map/all_to_all | solution.py:33
  288.3 2.1 copy.69
  290.4 7.0 %fusion.4 = bf16[192,2048]{1,0:T(8,128)(2,1)} fusion(bf16[2048,2048]{1,0:T(8,128)(2,1)} %all-gather.8.cloned.1.call-done, bf16[192,2048]{1,0:T(8,128)(2,1)} %bitcast.84), kind=kOutput, calls=%fused_computation.8 | convolution fusion | flops 1611988992 | bytes 9961472 | tf_op jit(solution)/shard_map/dot_general | solution.py:97
  297.4 2.1 copy.74
  299.5 62.6 %all-to-all-done.4 = bf16[64,48,512]{2,1,0:T(8,128)(2,1)S(1)} async-done(((bf16[64,48,512]{2,1,0:T(8,128)(2,1)}), bf16[64,48,512]{2,1,0:T(8,128)(2,1)S(1)}, u32[]{:S(2)}, u32[]{:S(2)}) %all-to-all-start.4) | async-done | bytes 3145760 | tf_op jit(solution)/shard_map/all_to_all | solution.py:33
  362.1 4.8 %all-to-all-start.6 = ((bf16[192,4,512]{2,0,1:T(8,128)(2,1)}), bf16[192,4,512]{2,0,1:T(8,128)(2,1)}, u32[]{:S(2)}, u32[]{:S(2)}) async-start(bf16[192,4,512]{2,0,1:T(8,128)(2,1)} %bitcast.81), calls=%async_computation.6 | async-start | bytes 1572864 | tf_op jit(solution)/shard_map/all_to_all | solution.py:100
  367.7 5.4 %gather_fusion = bf16[1536,512]{1,0:T(8,128)(2,1)} fusion(bf16[3072,512]{1,0:T(8,128)(2,1)S(1)} %bitcast.71, s32[2048]{0:T(1024)S(1)} %pad_clamp_fusion), kind=kCustom, calls=%fused_computation | custom fusion | bytes 3151872 | tf_op jit(solution)/shard_map/gather | solution.py:87
  373.1 3.4 reshape.96
  376.5 5.9 %multiply_reduce_fusion = f32[768,512]{1,0:T(8,128)} fusion(f32[768,2,512]{2,1,0:T(2,128)S(1)} %reshape.96, f32[768,2]{1,0:T(8,128)S(1)} %copy.64), kind=kLoop, calls=%fused_computation.7 | loop fusion | flops 1179648 | bytes 4724736 | tf_op jit(solution)/shard_map/reduce_sum | solution.py:90
  382.4 2.7 fusion.16
  (55 shorter events, 6.0 us)
Async XLA Ops:
  6.5 9.6 %copy-start.2 = (s32[768,2]{0,1:T(2,128)S(1)}, s32[768,2]{0,1:T(2,128)}, u32[]{:S(2)}) copy-start(s32[768,2]{0,1:T(2,128)} %param.12) | copy-start | bytes 18436
  6.5 170.8 %all-gather.10.cloned.1.call-start = ((), (), s32[]{:S(2)}) async-start(), calls=%async_computation.8 | async-start | bytes 2621440 | tf_op jit(solution)/shard_map/all_gather | solution.py:67
  7.3 174.7 %all-gather.12.cloned.1.call-start = ((), (), s32[]{:S(2)}) async-start(), calls=%async_computation.9 | async-start | bytes 2621440 | tf_op jit(solution)/shard_map/all_gather | solution.py:68
  10.0 26.5 %all-to-all-start = ((f32[4,1,768]{2,1,0:T(1,128)}), f32[4,1,768]{2,1,0:T(1,128)S(1)}, u32[]{:S(2)}, u32[]{:S(2)}) async-start(f32[4,1,768]{2,1,0:T(1,128)} %broadcast_in_dim.7), calls=%async_computation | async-start | bytes 24576 | tf_op jit(solution)/shard_map/all_to_all | solution.py:12
  15.4 166.5 %all-gather.14.cloned.1.call-start = ((), (), s32[]{:S(2)}) async-start(), calls=%async_computation.10 | async-start | bytes 2621440 | tf_op jit(solution)/shard_map/all_gather | solution.py:69
  35.0 1.6 copy-start.1
  35.0 1.6 copy-start.7
  36.8 0.9 copy-start
  48.7 11.7 %copy-start.3 = (bf16[256,32]{0,1:T(8,128)(2,1)S(1)}, bf16[256,32]{0,1:T(8,128)(2,1)}, u32[]{:S(2)}) copy-start(bf16[256,32]{0,1:T(8,128)(2,1)} %param.18) | copy-start | bytes 49156
  48.7 11.7 %copy-start.4 = (bf16[32,256]{1,0:T(8,128)(2,1)S(1)}, bf16[32,256]{1,0:T(8,128)(2,1)}, u32[]{:S(2)}) copy-start(bf16[32,256]{1,0:T(8,128)(2,1)} %param.17) | copy-start | bytes 49156
  48.7 85.5 %all-to-all-start.1 = ((bf16[64,48,512]{2,1,0:T(8,128)(2,1)}), bf16[64,48,512]{2,1,0:T(8,128)(2,1)S(1)}, u32[]{:S(2)}, u32[]{:S(2)}) async-start(bf16[64,48,512]{2,1,0:T(8,128)(2,1)} %bitcast.74), calls=%async_computation.1 | async-start | bytes 6291456 | tf_op jit(solution)/shard_map/all_to_all | solution.py:72
  60.3 230.1 %all-gather.8.cloned.1.call-start = ((), (), s32[]{:S(2)}) async-start(), calls=%async_computation.7 | async-start | bytes 8519680 | tf_op jit(solution)/shard_map/all_gather | solution.py:24
  254.0 25.0 %all-to-all-start.5 = ((bf16[4,192,512]{2,1,0:T(8,128)(2,1)}), bf16[4,192,512]{2,1,0:T(8,128)(2,1)}, u32[]{:S(2)}, u32[]{:S(2)}) async-start(bf16[4,192,512]{2,1,0:T(8,128)(2,1)} %bitcast.78), calls=%async_computation.5 | async-start | bytes 1572864 | tf_op jit(solution)/shard_map/all_to_all | solution.py:91
  279.1 83.1 %all-to-all-start.4 = ((bf16[64,48,512]{2,1,0:T(8,128)(2,1)}), bf16[64,48,512]{2,1,0:T(8,128)(2,1)S(1)}, u32[]{:S(2)}, u32[]{:S(2)}) async-start(bf16[64,48,512]{2,1,0:T(8,128)(2,1)} %bitcast.77), calls=%async_computation.4 | async-start | bytes 6291456 | tf_op jit(solution)/shard_map/all_to_all | solution.py:33
  297.4 69.5 %copy-start.8 = (f32[512]{0:T(512)S(1)}, f32[512]{0:T(512)}, u32[]{:S(2)}) copy-start(f32[512]{0:T(512)} %param.19) | copy-start | bytes 6148
  297.4 70.1 %copy-start.6 = (f32[768,2]{0,1:T(2,128)S(1)}, f32[768,2]{0,1:T(2,128)}, u32[]{:S(2)}) copy-start(f32[768,2]{0,1:T(2,128)} %param.13) | copy-start | bytes 18436
  362.1 20.3 %all-to-all-start.6 = ((bf16[192,4,512]{2,0,1:T(8,128)(2,1)}), bf16[192,4,512]{2,0,1:T(8,128)(2,1)}, u32[]{:S(2)}, u32[]{:S(2)}) async-start(bf16[192,4,512]{2,0,1:T(8,128)(2,1)} %bitcast.81), calls=%async_computation.6 | async-start | bytes 1572864 | tf_op jit(solution)/shard_map/all_to_all | solution.py:100
  376.5 5.9 %copy-start.5 = (f32[512]{0:T(512)S(1)}, f32[512]{0:T(512)}, u32[]{:S(2)}) copy-start(f32[512]{0:T(512)} %add_divide_fusion) | copy-start | bytes 6148
Sparse Core Ops, SparseCore 0:
  9.1 35.3 all-gather.9
  46.3 34.3 all-gather.11
  82.6 33.3 all-gather.13
  118.6 83.9 all-gather.7
where the time goes:
time: 393 us; the launch traced here: 392 us
  waiting for transfers between devices  125 us (32%)
  blocking collectives  91 us (23%)
  local copies, waits for them, and re-layouts  75.8 us (19%)
  starting transfers between devices  36.7 us (9%)
  other arithmetic  30.1 us (8%)
  matrix products  19.5 us (5%)
  between operations  13.4 us (3%)
    all_to_all x1, waiting for transfers between devices, send_back(): return lax.all_to_all(result, 'ep', split_axis=0, concat_axis=0, tiled=True)  62.6 us
    all_to_all x1, waiting for transfers between devices, body(): lax.all_to_all(buffer, 'ep', split_axis=0, concat_axis=0, tiled=True)  60.4 us
    all_to_all x1, blocking collectives, body(): lax.all_to_all(lax.all_to_all(buffer, 'ep', split_axis=0, concat_axis=0,...  39.5 us
    all_to_all x1, blocking collectives, body(): lax.all_to_all(result.reshape(row_split.shape), 'tp', split_axis=2, conca...  38.8 us
    unnamed x23, local copies, waits for them, and re-layouts  27 us
    another operation x3, other arithmetic  18.4 us
    all_gather x1, blocking collectives, gather_turned(): lax.all_gather(both, axis, axis=0, tiled=True)  12.7 us
    all_to_all x1, starting transfers between devices, body(): lax.all_to_all(buffer, 'ep', split_axis=0, concat_axis=0, tiled=True)  11.6 us
  transfers between devices with their start and end apart: 9, of which 2 were waited for; matrix products, arithmetic and copies ran while one was open for 31% of the time, Pallas kernels for 0%

commit v1 on v0

--- a/solution.py
+++ b/solution.py
@@ -80,8 +80,14 @@
     up_sum = jnp.dot(slot_rows, up_whole, preferred_element_type=jnp.float32)
     hidden = (jax.nn.silu(gate_sum) * up_sum).astype(jnp.bfloat16)
     result = jnp.dot(hidden, down_whole, preferred_element_type=jnp.float32).astype(jnp.bfloat16)
-    feature_split = lax.all_to_all(
-        result.reshape(row_split.shape), "tp", split_axis=2, concat_axis=0, tiled=True
+    feature_split = jnp.concatenate(
+        lax.all_to_all(
+            jnp.stack(jnp.split(result.reshape(row_split.shape), lax.axis_size("tp"), axis=2)),
+            "tp",
+            0,
+            0,
+        ),
+        axis=0,
     )
     returned = send_back(feature_split)
     picked = returned.reshape(expert_count * capacity, quarter)[position].reshape(

time: 393 us -> 352 us (0.90)
  local copies, waits for them, and re-layouts: 75.8 us -> 35.1 us
    unnamed x23 -> x21, local copies, waits for them, and re-layouts: 27 us -> 2.28 us
    reshape x1 -> x0, local copies, waits for them, and re-layouts: 10.5 us -> none  [body(): result.reshape(row_split.shape)]
    all_to_all x1 -> x0, local copies, waits for them, and re-layouts: 9.54 us -> none  [body(): lax.all_to_all(result.reshape(row_split.shape), 'tp', split_axis=2, conca...]
    another operation x3 -> x4, other arithmetic: 18.4 us -> 18.8 us
  transfers between devices with their start and end apart: 9 -> 9, of which waited for: 2 -> 2; matrix products, arithmetic and copies ran while one was open for 31% -> 23% of each run, Pallas kernels for 0% -> 0%
where the time goes in v1:
time: 352 us; the launch traced here: 351 us
  waiting for transfers between devices  125 us (36%)
  blocking collectives  90.2 us (26%)
  starting transfers between devices  37 us (11%)
  local copies, waits for them, and re-layouts  35.1 us (10%)
  other arithmetic  30.6 us (9%)
  matrix products  19.7 us (6%)
  between operations  13.4 us (4%)
    all_to_all x1, waiting for transfers between devices, send_back(): return lax.all_to_all(result, 'ep', split_axis=0, concat_axis=0, tiled=True)  62.7 us
    all_to_all x1, waiting for transfers between devices, body(): lax.all_to_all(buffer, 'ep', split_axis=0, concat_axis=0, tiled=True)  60.4 us
    all_to_all x1, blocking collectives, body(): lax.all_to_all(lax.all_to_all(buffer, 'ep', split_axis=0, concat_axis=0,...  39.6 us
    all_to_all x1, blocking collectives, body(): lax.all_to_all(jnp.stack(jnp.split(result.reshape(row_split.shape), lax.a...  37.9 us
    another operation x3, other arithmetic  18.4 us
    all_gather x1, blocking collectives, gather_turned(): lax.all_gather(both, axis, axis=0, tiled=True)  12.7 us
    all_to_all x1, starting transfers between devices, body(): lax.all_to_all(buffer, 'ep', split_axis=0, concat_axis=0, tiled=True)  11.6 us
    scatter x1, local copies, waits for them, and re-layouts, body(): jnp.zeros((expert_count * capacity, quarter), jnp.bfloat16).at[position]  9.5 us
  transfers between devices with their start and end apart: 9, of which 2 were waited for; matrix products, arithmetic and copies ran while one was open for 23% of the time, Pallas kernels for 0%

profile of v1, /device:TPU:2, one launch (start us, length us, event | category | flops | bytes accessed | tf_op | source)
XLA Modules:
  0.0 351.2 jit_solution(18400567840676134336)
XLA Ops:
  6.5 0.7 all-gather.10.cloned.1.call-update
  7.3 0.7 all-gather.12.cloned.1.call-update
  8.0 1.4 fusion.12
  10.0 5.5 %all-to-all-start = ((f32[4,1,768]{2,1,0:T(1,128)}), f32[4,1,768]{2,1,0:T(1,128)S(1)}, u32[]{:S(2)}, u32[]{:S(2)}) async-start(f32[4,1,768]{2,1,0:T(1,128)} %broadcast_in_dim.7), calls=%async_computation | async-start | bytes 24576 | tf_op jit(solution)/shard_map/all_to_all | solution.py:12
  15.4 0.7 all-gather.14.cloned.1.call-update
  16.9 18.1 %reduce-window.6 = s32[64,12,128]{2,1,0:T(8,128)S(1)} reduce-window(s32[64,12,128]{2,1,0:T(8,128)S(1)} %fusion.27, s32[]{:T(128)} %constant.6.clone.1), window={size=1x1x128 pad=0_0x0_0x127_0}, to_apply=%region_0.0 | reduce-window | flops 12484608 | bytes 786436 | tf_op jit(solution)/shard_map/reduce-window
  36.8 0.9 copy-done
  37.7 0.8 broadcast_in_dim.8
  38.5 0.6 reshape.114
  39.2 9.5 %scatter_custom_fusion = bf16[3072,512]{1,0:T(8,128)(2,1)} fusion(s32[1536]{0:T(1024)S(1)} %fusion.32, bf16[1536,512]{1,0:T(8,128)(2,1)S(1)} %reshape.114, bf16[]{:T(256)} %constant.8.clone.1), kind=kCustom, calls=%fused_computation.24 | custom fusion | bytes 3145730 | tf_op jit(solution)/shard_map/scatter | solution.py:64
  48.7 11.6 %all-to-all-start.1 = ((bf16[64,48,512]{2,1,0:T(8,128)(2,1)}), bf16[64,48,512]{2,1,0:T(8,128)(2,1)S(1)}, u32[]{:S(2)}, u32[]{:S(2)}) async-start(bf16[64,48,512]{2,1,0:T(8,128)(2,1)} %bitcast.75), calls=%async_computation.1 | async-start | bytes 6291456 | tf_op jit(solution)/shard_map/all_to_all | solution.py:72
  60.4 12.7 %all_gather.18 = bf16[1024,64]{0,1:T(8,128)(2,1)S(1)} all-gather(bf16[256,64]{0,1:T(8,128)(2,1)S(1)} %pad_maximum_fusion.2), channel_id=1, replica_groups=mesh['ep'=64,'tp'=4] {'tp'}, dimensions={0}, use_global_device_ids=true | all-gather | bytes 163840 | tf_op jit(solution)/shard_map/all_gather | solution.py:24
  73.1 0.7 pad_maximum_fusion.1
  73.8 60.4 %all-to-all-done.1 = bf16[64,48,512]{2,1,0:T(8,128)(2,1)S(1)} async-done(((bf16[64,48,512]{2,1,0:T(8,128)(2,1)}), bf16[64,48,512]{2,1,0:T(8,128)(2,1)S(1)}, u32[]{:S(2)}, u32[]{:S(2)}) %all-to-all-start.1) | async-done | bytes 3145760 | tf_op jit(solution)/shard_map/all_to_all | solution.py:72
  134.1 39.6 %all_to_all.68 = bf16[64,48,512]{2,1,0:T(8,128)(2,1)} all-to-all(bf16[64,48,512]{2,1,0:T(8,128)(2,1)S(1)} %all-to-all-done.1), channel_id=1, replica_groups=mesh['ep'=64,'tp'=4] {'tp'}, dimensions={0} | all-to-all | bytes 6291456 | tf_op jit(solution)/shard_map/all_to_all | solution.py:71
  173.7 5.6 %all-to-all-start.5 = ((bf16[4,192,512]{2,1,0:T(8,128)(2,1)}), bf16[4,192,512]{2,1,0:T(8,128)(2,1)}, u32[]{:S(2)}, u32[]{:S(2)}) async-start(bf16[4,192,512]{2,1,0:T(8,128)(2,1)} %bitcast.79), calls=%async_computation.5 | async-start | bytes 1572864 | tf_op jit(solution)/shard_map/all_to_all | solution.py:97
  179.3 4.6 %copy.54 = bf16[16,48,4,512]{3,2,1,0:T(4,128)(2,1)S(1)} copy(bf16[16,48,4,512]{3,1,0,2:T(8,128)(2,1)} %bitcast.77) | data formatting | bytes 6291456 | tf_op jit(solution)/shard_map/all_to_all | solution.py:71
  183.9 1.0 copy.62
  184.9 4.7 %fusion.10 = f32[768,512]{1,0:T(8,128)} fusion(bf16[768,2048]{1,0:T(8,128)(2,1)S(1)} %bitcast.80, bf16[1,2048,512]{2,1,0:T(8,128)(2,1)} %all-gather.10.cloned.1.call-done), kind=kOutput, calls=%fused_computation.13 | convolution fusion | flops 1610612736 | bytes 6815744 | tf_op jit(solution)/shard_map/dot_general | solution.py:79
  189.7 8.0 %convolution_convert_fusion = bf16[768,2048]{1,0:T(8,128)(2,1)} fusion(bf16[1,512,2048]{2,1,0:T(8,128)(2,1)} %all-gather.14.cloned.1.call-done, f32[768,512]{1,0:T(8,128)} %fusion.10, bf16[768,2048]{1,0:T(8,128)(2,1)S(1)} %bitcast.81, bf16[1,2048,512]{2,1,0:T(8,128)(2,1)} %all-gather.12.cloned.1.call-done), kind=kOutput, calls=%fused_computation.6 | convolution fusion | flops 3225157632 | bytes 12058624 | tf_op jit(solution)/shard_map/dot_general | solution.py:82
  197.7 2.2 slice_bitcast_fusion.3
  200.3 37.9 %all_to_all.69 = bf16[4,16,48,512]{3,2,1,0:T(8,128)(2,1)} all-to-all(bf16[4,16,48,512]{3,2,1,0:T(8,128)(2,1)S(1)} %pad_maximum_fusion), channel_id=1, replica_groups=mesh['ep'=64,'tp'=4] {'tp'}, dimensions={0} | all-to-all | bytes 6291456 | tf_op jit(solution)/shard_map/all_to_all | solution.py:84
  238.2 8.7 %all-to-all-start.4 = ((bf16[64,48,512]{2,1,0:T(8,128)(2,1)}), bf16[64,48,512]{2,1,0:T(8,128)(2,1)S(1)}, u32[]{:S(2)}, u32[]{:S(2)}) async-start(bf16[64,48,512]{2,1,0:T(8,128)(2,1)} %bitcast.76), calls=%async_computation.4 | async-start | bytes 6291456 | tf_op jit(solution)/shard_map/all_to_all | solution.py:33
  246.9 2.1 copy.60
  249.0 7.0 %fusion.4 = bf16[192,2048]{1,0:T(8,128)(2,1)} fusion(bf16[2048,2048]{1,0:T(8,128)(2,1)} %all-gather.8.cloned.1.call-done, bf16[192,2048]{1,0:T(8,128)(2,1)} %bitcast.85), kind=kOutput, calls=%fused_computation.9 | convolution fusion | flops 1611988992 | bytes 9961472 | tf_op jit(solution)/shard_map/dot_general | solution.py:103
  256.0 2.1 copy.65
  258.1 62.7 %all-to-all-done.4 = bf16[64,48,512]{2,1,0:T(8,128)(2,1)S(1)} async-done(((bf16[64,48,512]{2,1,0:T(8,128)(2,1)}), bf16[64,48,512]{2,1,0:T(8,128)(2,1)S(1)}, u32[]{:S(2)}, u32[]{:S(2)}) %all-to-all-start.4) | async-done | bytes 3145760 | tf_op jit(solution)/shard_map/all_to_all | solution.py:33
  320.8 5.6 %all-to-all-start.6 = ((bf16[192,4,512]{2,0,1:T(8,128)(2,1)}), bf16[192,4,512]{2,0,1:T(8,128)(2,1)}, u32[]{:S(2)}, u32[]{:S(2)}) async-start(bf16[192,4,512]{2,0,1:T(8,128)(2,1)} %bitcast.83), calls=%async_computation.6 | async-start | bytes 1572864 | tf_op jit(solution)/shard_map/all_to_all | solution.py:106
  327.1 5.4 %gather_fusion = bf16[1536,512]{1,0:T(8,128)(2,1)} fusion(bf16[3072,512]{1,0:T(8,128)(2,1)S(1)} %bitcast.74, s32[2048]{0:T(1024)S(1)} %pad_clamp_fusion), kind=kCustom, calls=%fused_computation | custom fusion | bytes 3151872 | tf_op jit(solution)/shard_map/gather | solution.py:93
  332.5 3.4 reshape.100
  336.0 5.9 %multiply_reduce_fusion = f32[768,512]{1,0:T(8,128)} fusion(f32[768,2,512]{2,1,0:T(2,128)S(1)} %reshape.100, f32[768,2]{1,0:T(8,128)S(1)} %copy.55), kind=kLoop, calls=%fused_computation.8 | loop fusion | flops 1179648 | bytes 4724736 | tf_op jit(solution)/shard_map/reduce_sum | solution.py:96
  341.9 2.7 fusion.16
  (53 shorter events, 4.4 us)
Async XLA Ops:
  6.5 9.6 %copy-start.2 = (s32[768,2]{0,1:T(2,128)S(1)}, s32[768,2]{0,1:T(2,128)}, u32[]{:S(2)}) copy-start(s32[768,2]{0,1:T(2,128)} %param.12) | copy-start | bytes 18436
  6.5 178.4 %all-gather.10.cloned.1.call-start = ((), (), s32[]{:S(2)}) async-start(), calls=%async_computation.8 | async-start | bytes 2621440 | tf_op jit(solution)/shard_map/all_gather | solution.py:67
  7.3 182.4 %all-gather.12.cloned.1.call-start = ((), (), s32[]{:S(2)}) async-start(), calls=%async_computation.9 | async-start | bytes 2621440 | tf_op jit(solution)/shard_map/all_gather | solution.py:68
  10.0 26.5 %all-to-all-start = ((f32[4,1,768]{2,1,0:T(1,128)}), f32[4,1,768]{2,1,0:T(1,128)S(1)}, u32[]{:S(2)}, u32[]{:S(2)}) async-start(f32[4,1,768]{2,1,0:T(1,128)} %broadcast_in_dim.7), calls=%async_computation | async-start | bytes 24576 | tf_op jit(solution)/shard_map/all_to_all | solution.py:12
  15.4 174.3 %all-gather.14.cloned.1.call-start = ((), (), s32[]{:S(2)}) async-start(), calls=%async_computation.10 | async-start | bytes 2621440 | tf_op jit(solution)/shard_map/all_gather | solution.py:69
  35.0 1.6 copy-start.1
  35.0 1.6 copy-start.7
  36.8 0.9 copy-start
  48.7 11.7 %copy-start.3 = (bf16[256,32]{0,1:T(8,128)(2,1)S(1)}, bf16[256,32]{0,1:T(8,128)(2,1)}, u32[]{:S(2)}) copy-start(bf16[256,32]{0,1:T(8,128)(2,1)} %param.18) | copy-start | bytes 49156
  48.7 11.7 %copy-start.4 = (bf16[32,256]{1,0:T(8,128)(2,1)S(1)}, bf16[32,256]{1,0:T(8,128)(2,1)}, u32[]{:S(2)}) copy-start(bf16[32,256]{1,0:T(8,128)(2,1)} %param.17) | copy-start | bytes 49156
  48.7 85.5 %all-to-all-start.1 = ((bf16[64,48,512]{2,1,0:T(8,128)(2,1)}), bf16[64,48,512]{2,1,0:T(8,128)(2,1)S(1)}, u32[]{:S(2)}, u32[]{:S(2)}) async-start(bf16[64,48,512]{2,1,0:T(8,128)(2,1)} %bitcast.75), calls=%async_computation.1 | async-start | bytes 6291456 | tf_op jit(solution)/shard_map/all_to_all | solution.py:72
  60.3 188.7 %all-gather.8.cloned.1.call-start = ((), (), s32[]{:S(2)}) async-start(), calls=%async_computation.7 | async-start | bytes 8519680 | tf_op jit(solution)/shard_map/all_gather | solution.py:24
  173.7 26.6 %all-to-all-start.5 = ((bf16[4,192,512]{2,1,0:T(8,128)(2,1)}), bf16[4,192,512]{2,1,0:T(8,128)(2,1)}, u32[]{:S(2)}, u32[]{:S(2)}) async-start(bf16[4,192,512]{2,1,0:T(8,128)(2,1)} %bitcast.79), calls=%async_computation.5 | async-start | bytes 1572864 | tf_op jit(solution)/shard_map/all_to_all | solution.py:97
  238.2 82.6 %all-to-all-start.4 = ((bf16[64,48,512]{2,1,0:T(8,128)(2,1)}), bf16[64,48,512]{2,1,0:T(8,128)(2,1)S(1)}, u32[]{:S(2)}, u32[]{:S(2)}) async-start(bf16[64,48,512]{2,1,0:T(8,128)(2,1)} %bitcast.76), calls=%async_computation.4 | async-start | bytes 6291456 | tf_op jit(solution)/shard_map/all_to_all | solution.py:33
  256.0 70.4 %copy-start.8 = (f32[512]{0:T(512)S(1)}, f32[512]{0:T(512)}, u32[]{:S(2)}) copy-start(f32[512]{0:T(512)} %param.19) | copy-start | bytes 6148
  256.0 71.0 %copy-start.6 = (f32[768,2]{0,1:T(2,128)S(1)}, f32[768,2]{0,1:T(2,128)}, u32[]{:S(2)}) copy-start(f32[768,2]{0,1:T(2,128)} %param.13) | copy-start | bytes 18436
  320.8 21.1 %all-to-all-start.6 = ((bf16[192,4,512]{2,0,1:T(8,128)(2,1)}), bf16[192,4,512]{2,0,1:T(8,128)(2,1)}, u32[]{:S(2)}, u32[]{:S(2)}) async-start(bf16[192,4,512]{2,0,1:T(8,128)(2,1)} %bitcast.83), calls=%async_computation.6 | async-start | bytes 1572864 | tf_op jit(solution)/shard_map/all_to_all | solution.py:106
  336.0 5.9 %copy-start.5 = (f32[512]{0:T(512)S(1)}, f32[512]{0:T(512)}, u32[]{:S(2)}) copy-start(f32[512]{0:T(512)} %add_divide_fusion) | copy-start | bytes 6148
Sparse Core Ops, SparseCore 0:
  9.1 35.3 all-gather.9
  46.3 34.3 all-gather.11
  82.6 33.3 all-gather.13
  118.6 83.9 all-gather.7
